TPU v7x, 32 devices: a whole 2x2x4 slice. The times are simulated.
32 devices in a mesh: ep: 8 (over z, x), tp: 4 (over y, core).
Axes of the slice: x: 2, y: 2, z: 4, core: 2. Of those that a mesh axis runs over, the one named last changes fastest.
Arguments:
- queries: bfloat16 [1024, 4096], P('ep', 'tp'), may hold values from -112 to 112
- key_rows: bfloat16 [1024, 4096], P('ep', 'tp'), may hold values from -8.1 to 8.1
- values: bfloat16 [1024, 4096], P('ep', 'tp'), may hold values from -6 to 6
- lambdas: float32 [16], P('tp'), may hold values from 0.3 to 0.8
- head_gain: float32 [256], replicated, may hold values from 0.1 to 1.9
- tokens: bfloat16 [512, 4096], P('ep'), may hold values from -6 to 6
- moe_gain: float32 [4096], replicated, may hold values from 0.1 to 1.9
- routes: int32 [512, 2], P('ep'), may hold values from 0 to 7, all different within a row; in each aligned block of 64 rows (0 to 63, 64 to 127, ...) at most 32 rows name the same one
- route_scores: float32 [512, 2], P('ep'), may hold values from -6 to 6
- w_gate: bfloat16 [8, 4096, 2048], P('ep', None, 'tp'), may hold values from -0.09375 to 0.09375
- w_up: bfloat16 [8, 4096, 2048], P('ep', None, 'tp'), may hold values from -0.09375 to 0.09375
- w_down: bfloat16 [8, 2048, 4096], P('ep', 'tp'), may hold values from -0.125 to 0.125
Outputs:
- attended: bfloat16 [1024, 4096], P('ep', 'tp')
- expert_out: bfloat16 [512, 4096], P('ep', 'tp')
Inputs may be any that keep to these rules, and one draw needn't show every extreme that they name: `routes`: each row names 2 different experts. Among the rows of one index of ep at most 32 name the same expert, and some index reaches 32 in every draw.
All inputs are finite; a program needn't handle non-finite values.
Results may differ from a plain program's by a relative error of at most 0.018.
Values may be sent and summed in bfloat16 or wider, within the bound.
A program may use at most 64 MiB of HBM per device.

v0:
```python
import jax
import jax.numpy as jnp
from jax import lax
from jax.sharding import PartitionSpec as P

QKD = 128
VD = 256
TOP = 2
neg_big = -1e30
head_eps = 1e-05
moe_eps = 1e-06
head_scale = 0.8


def slot_table(routes, experts, capacity):
    flat_routes = routes.reshape(-1)
    onehot = (flat_routes[:, None] == jnp.arange(experts, dtype=jnp.int32)[None, :]).astype(
        jnp.int32
    )
    before = jnp.cumsum(onehot, axis=0) - onehot
    position = jnp.sum(before * onehot, axis=1)
    return (flat_routes * capacity + position).reshape(routes.shape)


def fold_block(state, query_group, query_pos, key_heads, value_heads, key_pos):
    maxima, denominators, accumulated = state
    scores = jnp.einsum(
        "qhmd,khmd->hmqk", query_group, key_heads, preferred_element_type=jnp.float32
    ) * QKD ** (-0.5)
    visible = key_pos[None, :] <= query_pos[:, None]
    scores = jnp.where(visible, scores, neg_big)
    new_max = jnp.maximum(maxima, jnp.max(scores, axis=-1))
    weights = jnp.where(visible, jnp.exp(scores - new_max[..., None]), 0.0)
    accumulated = jnp.einsum(
        "hmqk,khd->hmqd", weights, value_heads, precision=lax.Precision.HIGHEST
    )
    denominators = jnp.sum(weights, axis=-1)
    return (new_max, denominators, accumulated)


def local(
    queries,
    key_rows,
    values,
    lambdas,
    head_gain,
    tokens,
    moe_gain,
    routes,
    route_scores,
    w_gate,
    w_up,
    w_down,
):
    rows_a = queries.shape[0]
    half_rows = rows_a // 2
    head_local = lambdas.shape[0]
    ep_count = lax.axis_size("ep")
    ep_index = lax.axis_index("ep")
    early_queries = queries[:half_rows]
    later_queries = queries[half_rows:]
    early_pos = ep_index * rows_a + jnp.arange(half_rows, dtype=jnp.int32)
    later_pos = ep_index * rows_a + half_rows + jnp.arange(half_rows, dtype=jnp.int32)
    query_groups = (
        early_queries.reshape(half_rows, head_local, 2, QKD),
        later_queries.reshape(half_rows, head_local, 2, QKD),
    )
    position_groups = (early_pos, later_pos)
    start_state = (
        jnp.full((head_local, 2, half_rows), neg_big, jnp.float32),
        jnp.zeros((head_local, 2, half_rows), jnp.float32),
        jnp.zeros((head_local, 2, half_rows, VD), jnp.float32),
    )
    totals = (start_state, start_state)
    row_start = jnp.int32(0)
    key_block = lax.all_gather(key_rows, "ep", axis=0, tiled=True)
    value_block = lax.all_gather(values, "ep", axis=0, tiled=True)
    key_count = key_block.shape[0]
    key_heads = key_block.reshape(key_count, head_local, 2, QKD)
    value_heads = value_block.reshape(key_count, head_local, VD).astype(jnp.float32)
    key_pos = jnp.arange(key_count, dtype=jnp.int32)
    updated = []
    for attend_group_index in range(2):
        state = totals[attend_group_index]
        query_group = query_groups[attend_group_index]
        query_pos = position_groups[attend_group_index]
        state = lax.cond(
            row_start <= query_pos[-1],
            lambda held: fold_block(held, query_group, query_pos, key_heads, value_heads, key_pos),
            lambda held: held,
            state,
        )
        updated.append(state)
    folded = (updated[0], updated[1])
    attended_groups = []
    for group_index in range(2):
        maxima, denominators, accumulated = folded[group_index]
        mixed_out = (
            accumulated[:, 0] / denominators[:, 0, :, None]
            - lambdas[:, None, None] * accumulated[:, 1] / denominators[:, 1, :, None]
        )
        scaled = mixed_out * lax.rsqrt(
            jnp.mean(mixed_out * mixed_out, axis=-1, keepdims=True) + head_eps
        )
        scaled = scaled * head_gain * head_scale
        attended_groups.append(
            scaled.transpose(1, 0, 2).reshape(half_rows, head_local * VD).astype(jnp.bfloat16)
        )
    later_out = attended_groups[1]
    attended = jnp.concatenate([attended_groups[0], later_out], axis=0)
    rows_b = tokens.shape[0]
    capacity = 2 * TOP * rows_b // ep_count
    token_f32 = tokens.astype(jnp.float32)
    normed = (
        token_f32
        * lax.rsqrt(jnp.mean(token_f32 * token_f32, axis=-1, keepdims=True) + moe_eps)
        * moe_gain
    ).astype(jnp.bfloat16)
    gate_weights = jax.nn.softmax(route_scores, axis=-1)
    slot_of = slot_table(routes, ep_count, capacity)
    row_ids = jnp.broadcast_to(jnp.arange(rows_b, dtype=jnp.int32)[:, None], slot_of.shape)
    row_of_slot = (
        jnp.zeros((ep_count * capacity,), jnp.int32)
        .at[slot_of.reshape(-1)]
        .set(row_ids.reshape(-1))
    )
    gate_local = w_gate[0]
    up_local = w_up[0]
    down_local = w_down[0]
    outgoing = normed[row_of_slot]
    arrived = lax.all_to_all(outgoing, "ep", split_axis=0, concat_axis=0, tiled=True)
    gate_act = jnp.dot(arrived, gate_local, preferred_element_type=jnp.float32)
    up_act = jnp.dot(arrived, up_local, preferred_element_type=jnp.float32)
    hidden = (jax.nn.silu(gate_act) * up_act).astype(jnp.bfloat16)
    summed = lax.psum_scatter(
        lax.dot_general(
            down_local, hidden, (((0,), (1,)), ((), ())), preferred_element_type=jnp.float32
        ).astype(jnp.bfloat16),
        "tp",
        scatter_dimension=0,
        tiled=True,
    )
    returned = lax.all_to_all(summed, "ep", split_axis=1, concat_axis=1, tiled=True)
    slot_ids = jnp.arange(ep_count * capacity, dtype=jnp.int32)
    combined = jnp.zeros((rows_b, returned.shape[0]), jnp.float32)
    for choice_index in range(TOP):
        picker = (slot_of[:, choice_index, None] == slot_ids[None, :]).astype(jnp.bfloat16)
        picked = lax.dot_general(
            picker, returned, (((1,), (1,)), ((), ())), preferred_element_type=jnp.float32
        )
        combined = combined + gate_weights[:, choice_index, None] * picked
    expert_out = combined.astype(jnp.bfloat16)
    return (attended, expert_out)


def solution(mesh):
    return jax.shard_map(
        local,
        mesh=mesh,
        in_specs=(
            P("ep", "tp"),
            P("ep", "tp"),
            P("ep", "tp"),
            P("tp"),
            P(),
            P("ep", None),
            P(),
            P("ep", None),
            P("ep", None),
            P("ep", None, "tp"),
            P("ep", None, "tp"),
            P("ep", "tp", None),
        ),
        out_specs=(P("ep", "tp"), P("ep", "tp")),
        check_vma=False,
    )
```

profile of v0, /device:TPU:0, one launch (start us, length us, event | category | flops | bytes accessed | tf_op | source)
XLA Modules:
  0.0 190.7 jit_solution(13893074613434656306)
XLA Ops:
  8.0 0.0 copy-start.2
  8.0 0.0 all-gather.5.cloned.1.call-start
  8.1 1.9 copy.24
  9.9 0.0 all-gather.5.cloned.1.call-update
  9.9 0.8 copy.34
  10.7 0.1 eq.45
  10.8 0.1 fusion.62
  10.9 0.2 reduce_window_sum.11
  11.1 0.2 select_reduce_fusion
  11.3 0.1 reduce_sum.71
  11.5 0.1 mul.157
  11.6 0.1 reshape.129
  11.8 1.0 scatter_custom_fusion
  12.8 1.2 fusion.42
  14.0 0.0 copy-done.2
  14.0 0.9 fusion.44
  15.0 3.2 %gather_fusion = bf16[256,4096]{1,0:T(8,128)(2,1)} fusion(bf16[64,4096]{1,0:T(8,128)(2,1)S(1)} %fusion.44, s32[1024]{0:T(1024)S(1)} %pad_clamp_fusion), kind=kCustom, calls=%fused_computation | custom fusion | bytes 4195328 | tf_op jit(solution)/shard_map/gather | solution.py:130
  18.2 7.4 %all-to-all-start = ((bf16[8,32,4096]{2,1,0:T(8,128)(2,1)}), bf16[8,32,4096]{2,1,0:T(8,128)(2,1)S(1)}, u32[]{:S(2)}, u32[]{:S(2)}) async-start(bf16[8,32,4096]{2,1,0:T(8,128)(2,1)} %bitcast.20), calls=%async_computation | async-start | bytes 4194304 | tf_op jit(solution)/shard_map/all_to_all | solution.py:131
  25.6 0.0 all-gather.3.cloned.1.call-start
  25.6 0.0 copy-done.3
  25.6 0.8 copy.23
  26.5 0.0 all-gather.3.cloned.1.call-update
  26.5 0.0 reduce-scatter.2.cloned.1.call-start
  26.5 69.8 %all-to-all-done = bf16[8,32,4096]{2,1,0:T(8,128)(2,1)S(1)} async-done(((bf16[8,32,4096]{2,1,0:T(8,128)(2,1)}), bf16[8,32,4096]{2,1,0:T(8,128)(2,1)S(1)}, u32[]{:S(2)}, u32[]{:S(2)}) %all-to-all-start) | async-done | bytes 2097184 | tf_op jit(solution)/shard_map/all_to_all | solution.py:131
  96.3 3.5 %fusion.32 = f32[256,512]{1,0:T(8,128)S(1)} fusion(bf16[256,4096]{1,0:T(8,128)(2,1)S(1)} %bitcast.99, bf16[1,4096,512]{2,1,0:T(8,128)(2,1)} %param.25), kind=kOutput, calls=%fused_computation.43 | convolution fusion | flops 1073741824 | bytes 6815744 | tf_op jit(solution)/shard_map/dot_general | solution.py:132
  99.8 7.4 %fusion.28 = bf16[4096,256]{0,1:T(8,128)(2,1)} fusion(bf16[1,512,4096]{2,1,0:T(8,128)(2,1)} %param.27, bf16[256,4096]{1,0:T(8,128)(2,1)S(1)} %bitcast.100, bf16[1,4096,512]{2,1,0:T(8,128)(2,1)} %param.26, f32[256,512]{1,0:T(8,128)S(1)} %fusion.32), kind=kOutput, calls=%fused_computation.39 | convolution fusion | flops 2149318656 | bytes 13107200 | tf_op jit(solution)/shard_map/dot_general | solution.py:136
  107.2 0.0 copy-start.5
  107.2 0.0 reduce-scatter.2.cloned.1.call-update
  107.2 0.6 slice.55
  108.5 0.6 slice.50
  109.7 0.0 copy-done.5
  109.8 0.2 slice_reduce_fusion
  110.0 0.0 all-gather.5.cloned.1.call-done
  110.0 0.0 copy-start.4
  110.0 4.1 %convert.3 = f32[1024,4,256]{0,2,1:T(8,128)} convert(bf16[1024,4,256]{0,2,1:T(8,128)(2,1)} %bitcast.98) | non-fusion elementwise | flops 1048576 | bytes 6291456 | tf_op jit(solution)/shard_map/convert_element_type | solution.py:80
  114.1 33.2 %all-gather.3.cloned.1.call-done = bf16[1024,1024]{0,1:T(8,128)(2,1)} async-done(((bf16[128,1024]{0,1:T(8,128)(2,1)}), bf16[1024,1024]{0,1:T(8,128)(2,1)}) %all-gather.3.cloned.1.call-update) | async-done | bytes 2097168 | tf_op jit(solution)/shard_map/all_gather | solution.py:76
  147.3 0.0 copy-done.4
  147.3 8.6 %conditional.3 = (f32[4,2,64]{2,1,0:T(2,128)S(1)}, f32[4,2,64,256]{3,2,1,0:T(8,128)S(1)}) conditional(s32[]{:T(128)} %bitcast.10, () %tuple.26, (s32[1024]{0:T(1024)S(1)}, s32[64]{0:T(128)S(1)}, bf16[128,1024]{1,0:T(8,128)(2,1)S(1)}, bf16[1024,4,2,128]{0,3,2,1:T(8,128)(2,1)}, f32[1024,4,256]{0,2,1:T(8,128)}) %tuple.56), branch_computations={%region_5.6_spmd, %region_6.9_spmd} | conditional | flops 1751186944 | bytes 30818604 | solution.py:87
  147.3 0.1 broadcast_compare_fusion.1
  147.4 0.1 reshape.109
  147.5 0.0 copy-start
  147.5 2.4 %fusion.16 = (f32[4,2,64]{2,1,0:T(2,128)S(1)}, f32[4,2,64,1024]{3,2,1,0:T(8,128)S(1)}) fusion(pred[64,1024]{1,0:T(8,128)(4,1)S(1)} %broadcast_compare_fusion.1, bf16[1024,4,2,128]{0,3,2,1:T(8,128)(2,1)} %get-tuple-element.52, bf16[64,4,2,128]{3,2,1,0:T(2,128)(2,1)S(1)} %reshape.109), kind=kOutput, calls=%fused_computation.24 | convolution fusion | flops 135790080 | bytes 4392960 | tf_op jit(solution)/shard_map/cond/branch_1_fun/qhmd,khmd->hmqk/dot_general | solution.py:27
  150.0 0.4 copy-done
  150.3 4.8 %fusion.14 = f32[4,2,64,256]{3,2,1,0:T(8,128)S(1)} fusion(f32[1024,4,256]{0,2,1:T(8,128)S(1)} %copy-done, f32[4,2,64,1024]{3,2,1,0:T(8,128)S(1)} %get-tuple-element.63, f32[4,2,64]{2,1,0:T(2,128)S(1)} %broadcast_maximum_fusion.1, pred[64,1024]{1,0:T(8,128)(4,1)S(1)} %broadcast_compare_fusion.1), kind=kOutput, calls=%fused_computation.20 | convolution fusion | flops 1612709888 | bytes 6883328 | tf_op jit(solution)/shard_map/cond/branch_1_fun/hmqk,khd->hmqd/dot_general | solution.py:34
  155.2 0.7 fusion.17
  155.9 0.0 copy-start.7
  155.9 8.8 %conditional.2 = (f32[4,2,64]{2,1,0:T(2,128)S(1)}, f32[4,2,64,256]{3,2,1,0:T(8,128)S(1)}) conditional(s32[]{:T(128)} %bitcast.2, () %tuple.24, (s32[1024]{0:T(1024)S(1)}, s32[64]{0:T(128)S(1)}, bf16[128,1024]{1,0:T(8,128)(2,1)S(1)}, bf16[1024,4,2,128]{0,3,2,1:T(8,128)(2,1)}, f32[1024,4,256]{0,2,1:T(8,128)}) %tuple.57), branch_computations={%region_0.0_spmd, %region_1.4_spmd} | conditional | flops 1751186944 | bytes 30818604 | solution.py:87
  156.1 0.1 broadcast_compare_fusion
  156.2 0.1 reshape.108
  156.3 0.0 copy-start.1
  156.3 2.4 %fusion.2 = (f32[4,2,64]{2,1,0:T(2,128)S(1)}, f32[4,2,64,1024]{3,2,1,0:T(8,128)S(1)}) fusion(pred[64,1024]{1,0:T(8,128)(4,1)S(1)} %broadcast_compare_fusion, bf16[1024,4,2,128]{0,3,2,1:T(8,128)(2,1)} %get-tuple-element.47, bf16[64,4,2,128]{3,2,1,0:T(2,128)(2,1)S(1)} %reshape.108), kind=kOutput, calls=%fused_computation.6 | convolution fusion | flops 135790080 | bytes 4392960 | tf_op jit(solution)/shard_map/cond/branch_1_fun/qhmd,khmd->hmqk/dot_general | solution.py:27
  158.7 0.4 copy-done.1
  159.1 4.8 %fusion = f32[4,2,64,256]{3,2,1,0:T(8,128)S(1)} fusion(f32[1024,4,256]{0,2,1:T(8,128)S(1)} %copy-done.1, f32[4,2,64,1024]{3,2,1,0:T(8,128)S(1)} %get-tuple-element.61, f32[4,2,64]{2,1,0:T(2,128)S(1)} %broadcast_maximum_fusion, pred[64,1024]{1,0:T(8,128)(4,1)S(1)} %broadcast_compare_fusion), kind=kOutput, calls=%fused_computation.2 | convolution fusion | flops 1612709888 | bytes 6883328 | tf_op jit(solution)/shard_map/cond/branch_1_fun/hmqk,khd->hmqd/dot_general | solution.py:34
  164.0 0.7 fusion.3
  164.7 0.0 reduce-scatter.2.cloned.1.call-done
  164.7 3.5 %all-to-all-start.1 = ((bf16[1024,8,32]{0,2,1:T(8,128)(2,1)}), bf16[1024,8,32]{0,2,1:T(8,128)(2,1)S(1)}, u32[]{:S(2)}, u32[]{:S(2)}) async-start(bf16[1024,8,32]{0,2,1:T(8,128)(2,1)} %bitcast.101), calls=%async_computation.2 | async-start | bytes 1048576 | tf_op jit(solution)/shard_map/all_to_all | solution.py:143
  168.2 0.0 copy-done.7
  168.3 0.4 multiply_reduce_fusion.1
  168.6 0.0 copy-done.6
  168.6 0.1 fusion.60
  168.8 0.7 pad_maximum_fusion
  169.5 12.6 %all-to-all-done.1 = bf16[1024,8,32]{0,2,1:T(8,128)(2,1)S(1)} async-done(((bf16[1024,8,32]{0,2,1:T(8,128)(2,1)}), bf16[1024,8,32]{0,2,1:T(8,128)(2,1)S(1)}, u32[]{:S(2)}, u32[]{:S(2)}) %all-to-all-start.1) | async-done | bytes 524320 | tf_op jit(solution)/shard_map/all_to_all | solution.py:143
  182.1 0.2 convolution_multiply_fusion.1
  182.4 0.9 fusion.41
  (25 shorter events, 0.2 us)
Async XLA Ops:
  8.0 6.0 %copy-start.2 = (bf16[64,4096]{1,0:T(8,128)(2,1)S(1)}, bf16[64,4096]{1,0:T(8,128)(2,1)}, u32[]{:S(2)}) copy-start(bf16[64,4096]{1,0:T(8,128)(2,1)} %param.21) | copy-start | bytes 1572868
  8.0 102.0 %all-gather.5.cloned.1.call-start = ((), (), s32[]{:S(2)}) async-start(), calls=%async_computation.4 | async-start | bytes 2359296 | tf_op jit(solution)/shard_map/all_gather | solution.py:77
  18.2 7.5 %copy-start.3 = (bf16[128,1024]{1,0:T(8,128)(2,1)S(1)}, bf16[128,1024]{1,0:T(8,128)(2,1)}, u32[]{:S(2)}) copy-start(bf16[128,1024]{1,0:T(8,128)(2,1)} %param.17) | copy-start | bytes 786436
  18.2 78.2 %all-to-all-start = ((bf16[8,32,4096]{2,1,0:T(8,128)(2,1)}), bf16[8,32,4096]{2,1,0:T(8,128)(2,1)S(1)}, u32[]{:S(2)}, u32[]{:S(2)}) async-start(bf16[8,32,4096]{2,1,0:T(8,128)(2,1)} %bitcast.20), calls=%async_computation | async-start | bytes 4194304 | tf_op jit(solution)/shard_map/all_to_all | solution.py:131
  25.6 121.7 %all-gather.3.cloned.1.call-start = ((), (), s32[]{:S(2)}) async-start(), calls=%async_computation.3 | async-start | bytes 2359296 | tf_op jit(solution)/shard_map/all_gather | solution.py:76
  26.5 138.2 %reduce-scatter.2.cloned.1.call-start = ((), (), s32[]{:S(2)}) async-start(), calls=%async_computation.5 | async-start | bytes 2621440 | tf_op jit(solution)/shard_map/reduce_scatter | solution.py:135
  107.2 2.5 %copy-start.5 = (f32[64,2]{0,1:T(2,128)S(1)}, f32[64,2]{0,1:T(2,128)}, u32[]{:S(2)}) copy-start(f32[64,2]{0,1:T(2,128)} %param.24) | copy-start | bytes 1540
  110.0 37.3 %copy-start.4 = (bf16[128,1024]{1,0:T(8,128)(2,1)S(1)}, bf16[128,1024]{1,0:T(8,128)(2,1)}, u32[]{:S(2)}) copy-start(bf16[128,1024]{1,0:T(8,128)(2,1)} %param.16) | copy-start | bytes 786436
  147.5 2.8 %copy-start = (f32[1024,4,256]{0,2,1:T(8,128)S(1)}, f32[1024,4,256]{0,2,1:T(8,128)}, u32[]{:S(2)}) copy-start(f32[1024,4,256]{0,2,1:T(8,128)} %get-tuple-element.53) | copy-start | bytes 12582916 | tf_op jit(solution)/shard_map/cond
  155.9 12.4 %copy-start.7 = (f32[4]{0:T(128)S(1)}, f32[4]{0:T(128)}, u32[]{:S(2)}) copy-start(f32[4]{0:T(128)} %param.19) | copy-start | bytes 52
  156.3 2.8 %copy-start.1 = (f32[1024,4,256]{0,2,1:T(8,128)S(1)}, f32[1024,4,256]{0,2,1:T(8,128)}, u32[]{:S(2)}) copy-start(f32[1024,4,256]{0,2,1:T(8,128)} %get-tuple-element.48) | copy-start | bytes 12582916 | tf_op jit(solution)/shard_map/cond
  164.7 4.0 %copy-start.6 = (f32[256]{0:T(256)S(1)}, f32[256]{0:T(256)}, u32[]{:S(2)}) copy-start(f32[256]{0:T(256)} %param.20) | copy-start | bytes 3076
  164.7 17.4 %all-to-all-start.1 = ((bf16[1024,8,32]{0,2,1:T(8,128)(2,1)}), bf16[1024,8,32]{0,2,1:T(8,128)(2,1)S(1)}, u32[]{:S(2)}, u32[]{:S(2)}) async-start(bf16[1024,8,32]{0,2,1:T(8,128)(2,1)} %bitcast.101), calls=%async_computation.2 | async-start | bytes 1048576 | tf_op jit(solution)/shard_map/all_to_all | solution.py:143
Sparse Core Ops, SparseCore 0:
  10.9 83.9 all-gather.4
  97.5 49.7 all-gather.2
Sparse Core Ops, SparseCore 1:
  107.3 30.1 reduce-scatter.1
where the time goes:
time: 191 us
  waiting for transfers between devices  116 us (61%)
  matrix products  26.5 us (14%)
  between operations  17.1 us (9%)
  starting transfers between devices  11 us (6%)
  local copies, waits for them, and re-layouts  10.5 us (5%)
  other arithmetic  9.63 us (5%)
    all_to_all x1, waiting for transfers between devices, local(): lax.all_to_all(outgoing, 'ep', split_axis=0, concat_axis=0, tiled=True)  69.8 us
    all_gather x1, waiting for transfers between devices, local(): key_block = lax.all_gather(key_rows, 'ep', axis=0, tiled=True)  33.2 us
    all_to_all x1, waiting for transfers between devices, local(): lax.all_to_all(summed, 'ep', split_axis=1, concat_axis=1, tiled=True)  12.6 us
    dot_general x2, matrix products, fold_block(): jnp.einsum('hmqk,khd->hmqd', weights, value_heads, precision=lax.Precisio...  9.67 us
    all_to_all x1, starting transfers between devices, local(): lax.all_to_all(outgoing, 'ep', split_axis=0, concat_axis=0, tiled=True)  7.41 us
    dot_general x1, matrix products, local(): lax.dot_general(down_local, hidden, (((0,), (1,)), ((), ())), preferred_e...  7.37 us
    dot_general x2, matrix products, fold_block(): jnp.einsum('qhmd,khmd->hmqk', query_group, key_heads, preferred_element_t...  4.85 us
    convert_element_type x1, other arithmetic, local(): value_block.reshape(key_count, head_local, VD).astype(jnp.float32)  4.08 us
  transfers between devices with their start and end apart: 5, of which 3 were waited for; matrix products, arithmetic and copies ran while one was open for 22% of the time, Pallas kernels for 0%

commit v1 on v0

--- a/solution.py
+++ b/solution.py
@@ -140,7 +140,15 @@
         scatter_dimension=0,
         tiled=True,
     )
-    returned = lax.all_to_all(summed, "ep", split_axis=1, concat_axis=1, tiled=True)
+    returned = jnp.concatenate(
+        lax.all_to_all(
+            jnp.stack(jnp.split(summed, lax.axis_size("ep"), 1), 0),
+            split_axis=0,
+            concat_axis=0,
+            axis_name="ep",
+        ),
+        1,
+    )
     slot_ids = jnp.arange(ep_count * capacity, dtype=jnp.int32)
     combined = jnp.zeros((rows_b, returned.shape[0]), jnp.float32)
     for choice_index in range(TOP):

time: 191 us -> 203 us (1.063)
  local copies, waits for them, and re-layouts: 10.5 us -> 21.5 us
    unnamed x15 -> x22, local copies, waits for them, and re-layouts: 3.5 us -> 13.7 us
  transfers between devices with their start and end apart: 5 -> 5, of which waited for: 3 -> 3; matrix products, arithmetic and copies ran while one was open for 22% -> 21% of each run, Pallas kernels for 0% -> 0%
where the time goes in v1:
time: 203 us; the launch traced here: 202 us
  waiting for transfers between devices  116 us (57%)
  matrix products  26.3 us (13%)
  local copies, waits for them, and re-layouts  21.5 us (11%)
  between operations  17.1 us (8%)
  starting transfers between devices  11 us (5%)
  other arithmetic  9.62 us (5%)
    all_to_all x1, waiting for transfers between devices, local(): lax.all_to_all(outgoing, 'ep', split_axis=0, concat_axis=0, tiled=True)  69.8 us
    all_gather x1, waiting for transfers between devices, local(): key_block = lax.all_gather(key_rows, 'ep', axis=0, tiled=True)  33.5 us
    unnamed x22, local copies, waits for them, and re-layouts  13.7 us
    all_to_all x1, waiting for transfers between devices, local(): lax.all_to_all(jnp.stack(jnp.split(summed, lax.axis_size('ep'), 1), 0), s...  12.6 us
    dot_general x2, matrix products, fold_block(): jnp.einsum('hmqk,khd->hmqd', weights, value_heads, precision=lax.Precisio...  9.67 us
    all_to_all x1, starting transfers between devices, local(): lax.all_to_all(outgoing, 'ep', split_axis=0, concat_axis=0, tiled=True)  7.41 us
    dot_general x1, matrix products, local(): lax.dot_general(down_local, hidden, (((0,), (1,)), ((), ())), preferred_e...  7.24 us
    dot_general x2, matrix products, fold_block(): jnp.einsum('qhmd,khmd->hmqk', query_group, key_heads, preferred_element_t...  4.85 us
  transfers between devices with their start and end apart: 5, of which 3 were waited for; matrix products, arithmetic and copies ran while one was open for 21% of the time, Pallas kernels for 0%

profile of v1, /device:TPU:0, one launch (start us, length us, event | category | flops | bytes accessed | tf_op | source)
XLA Modules:
  0.0 201.8 jit_solution(14192604960678532009)
XLA Ops:
  8.0 0.0 copy-start.2
  8.0 0.0 all-gather.5.cloned.1.call-start
  8.1 1.8 copy.24
  9.9 0.0 all-gather.5.cloned.1.call-update
  9.9 0.8 copy.34
  10.7 0.1 eq.45
  10.8 0.1 fusion.70
  10.9 0.2 reduce_window_sum.11
  11.1 0.2 select_reduce_fusion
  11.3 0.1 reduce_sum.71
  11.4 0.1 mul.157
  11.6 0.1 reshape.135
  11.7 1.0 scatter_custom_fusion
  12.7 1.2 fusion.42
  14.0 0.9 fusion.44
  14.9 3.2 %gather_fusion = bf16[256,4096]{1,0:T(8,128)(2,1)} fusion(bf16[64,4096]{1,0:T(8,128)(2,1)S(1)} %fusion.44, s32[1024]{0:T(1024)S(1)} %pad_clamp_fusion), kind=kCustom, calls=%fused_computation | custom fusion | bytes 4195328 | tf_op jit(solution)/shard_map/gather | solution.py:130
  18.1 7.4 %all-to-all-start = ((bf16[8,32,4096]{2,1,0:T(8,128)(2,1)}), bf16[8,32,4096]{2,1,0:T(8,128)(2,1)S(1)}, u32[]{:S(2)}, u32[]{:S(2)}) async-start(bf16[8,32,4096]{2,1,0:T(8,128)(2,1)} %bitcast.20), calls=%async_computation | async-start | bytes 4194304 | tf_op jit(solution)/shard_map/all_to_all | solution.py:131
  25.5 0.0 all-gather.3.cloned.1.call-start
  25.6 0.8 copy.23
  26.4 0.0 all-gather.3.cloned.1.call-update
  26.5 0.0 reduce-scatter.2.cloned.1.call-start
  26.5 69.8 %all-to-all-done = bf16[8,32,4096]{2,1,0:T(8,128)(2,1)S(1)} async-done(((bf16[8,32,4096]{2,1,0:T(8,128)(2,1)}), bf16[8,32,4096]{2,1,0:T(8,128)(2,1)S(1)}, u32[]{:S(2)}, u32[]{:S(2)}) %all-to-all-start) | async-done | bytes 2097184 | tf_op jit(solution)/shard_map/all_to_all | solution.py:131
  96.3 3.4 %fusion.32 = f32[256,512]{1,0:T(8,128)S(1)} fusion(bf16[256,4096]{1,0:T(8,128)(2,1)S(1)} %bitcast.132, bf16[1,4096,512]{2,1,0:T(8,128)(2,1)} %param.25), kind=kOutput, calls=%fused_computation.43 | convolution fusion | flops 1073741824 | bytes 6815744 | tf_op jit(solution)/shard_map/dot_general | solution.py:132
  99.7 7.2 %fusion.28 = bf16[4096,256]{0,1:T(8,128)(2,1)} fusion(bf16[1,512,4096]{2,1,0:T(8,128)(2,1)} %param.27, bf16[256,4096]{1,0:T(8,128)(2,1)S(1)} %bitcast.133, bf16[1,4096,512]{2,1,0:T(8,128)(2,1)} %param.26, f32[256,512]{1,0:T(8,128)S(1)} %fusion.32), kind=kOutput, calls=%fused_computation.39 | convolution fusion | flops 2149318656 | bytes 13107200 | tf_op jit(solution)/shard_map/dot_general | solution.py:136
  107.0 0.0 reduce-scatter.2.cloned.1.call-update
  107.0 0.6 slice.50
  108.2 0.6 slice.55
  109.6 0.2 slice_reduce_fusion
  109.8 0.0 all-gather.5.cloned.1.call-done
  109.8 0.0 copy-start.4
  109.8 4.1 %convert.3 = f32[1024,4,256]{0,2,1:T(8,128)} convert(bf16[1024,4,256]{0,2,1:T(8,128)(2,1)} %bitcast.131) | non-fusion elementwise | flops 1048576 | bytes 6291456 | tf_op jit(solution)/shard_map/convert_element_type | solution.py:80
  113.9 33.5 %all-gather.3.cloned.1.call-done = bf16[1024,1024]{0,1:T(8,128)(2,1)} async-done(((bf16[128,1024]{0,1:T(8,128)(2,1)}), bf16[1024,1024]{0,1:T(8,128)(2,1)}) %all-gather.3.cloned.1.call-update) | async-done | bytes 2097168 | tf_op jit(solution)/shard_map/all_gather | solution.py:76
  147.5 0.0 copy-done.4
  147.5 8.2 %conditional.2 = (f32[4,2,64]{2,1,0:T(2,128)S(1)}, f32[4,2,64,256]{3,2,1,0:T(8,128)S(1)}) conditional(s32[]{:T(128)} %bitcast.2, () %tuple.24, (s32[1024]{0:T(1024)S(1)}, s32[64]{0:T(128)S(1)}, bf16[128,1024]{1,0:T(8,128)(2,1)S(1)}, bf16[1024,4,2,128]{0,3,2,1:T(8,128)(2,1)}, f32[1024,4,256]{0,2,1:T(8,128)}) %tuple.56), branch_computations={%region_0.0_spmd, %region_1.4_spmd} | conditional | flops 1751186944 | bytes 30818604 | solution.py:87
  147.5 0.1 broadcast_compare_fusion
  147.6 0.1 reshape.110
  147.7 0.0 copy-start
  147.7 2.4 %fusion.2 = (f32[4,2,64]{2,1,0:T(2,128)S(1)}, f32[4,2,64,1024]{3,2,1,0:T(8,128)S(1)}) fusion(pred[64,1024]{1,0:T(8,128)(4,1)S(1)} %broadcast_compare_fusion, bf16[1024,4,2,128]{0,3,2,1:T(8,128)(2,1)} %get-tuple-element.47, bf16[64,4,2,128]{3,2,1,0:T(2,128)(2,1)S(1)} %reshape.110), kind=kOutput, calls=%fused_computation.6 | convolution fusion | flops 135790080 | bytes 4392960 | tf_op jit(solution)/shard_map/cond/branch_1_fun/qhmd,khmd->hmqk/dot_general | solution.py:27
  150.1 0.7 fusion.3
  150.8 4.8 %fusion = f32[4,2,64,256]{3,2,1,0:T(8,128)S(1)} fusion(f32[1024,4,256]{0,2,1:T(8,128)S(1)} %copy-done, f32[4,2,64,1024]{3,2,1,0:T(8,128)S(1)} %get-tuple-element.61, f32[4,2,64]{2,1,0:T(2,128)S(1)} %broadcast_maximum_fusion, pred[64,1024]{1,0:T(8,128)(4,1)S(1)} %broadcast_compare_fusion), kind=kOutput, calls=%fused_computation.2 | convolution fusion | flops 1612709888 | bytes 6883328 | tf_op jit(solution)/shard_map/cond/branch_1_fun/hmqk,khd->hmqd/dot_general | solution.py:34
  155.7 8.4 %conditional.3 = (f32[4,2,64]{2,1,0:T(2,128)S(1)}, f32[4,2,64,256]{3,2,1,0:T(8,128)S(1)}) conditional(s32[]{:T(128)} %bitcast.10, () %tuple.26, (s32[1024]{0:T(1024)S(1)}, s32[64]{0:T(128)S(1)}, bf16[128,1024]{1,0:T(8,128)(2,1)S(1)}, bf16[1024,4,2,128]{0,3,2,1:T(8,128)(2,1)}, f32[1024,4,256]{0,2,1:T(8,128)}) %tuple.57), branch_computations={%region_5.6_spmd, %region_6.9_spmd} | conditional | flops 1751186944 | bytes 30818604 | solution.py:87
  155.9 0.1 broadcast_compare_fusion.1
  156.0 0.1 reshape.111
  156.1 2.4 %fusion.16 = (f32[4,2,64]{2,1,0:T(2,128)S(1)}, f32[4,2,64,1024]{3,2,1,0:T(8,128)S(1)}) fusion(pred[64,1024]{1,0:T(8,128)(4,1)S(1)} %broadcast_compare_fusion.1, bf16[1024,4,2,128]{0,3,2,1:T(8,128)(2,1)} %get-tuple-element.52, bf16[64,4,2,128]{3,2,1,0:T(2,128)(2,1)S(1)} %reshape.111), kind=kOutput, calls=%fused_computation.24 | convolution fusion | flops 135790080 | bytes 4392960 | tf_op jit(solution)/shard_map/cond/branch_1_fun/qhmd,khmd->hmqk/dot_general | solution.py:27
  158.5 0.7 fusion.17
  159.3 4.8 %fusion.14 = f32[4,2,64,256]{3,2,1,0:T(8,128)S(1)} fusion(f32[1024,4,256]{0,2,1:T(8,128)S(1)} %copy-done.1, f32[4,2,64,1024]{3,2,1,0:T(8,128)S(1)} %get-tuple-element.63, f32[4,2,64]{2,1,0:T(2,128)S(1)} %broadcast_maximum_fusion.1, pred[64,1024]{1,0:T(8,128)(4,1)S(1)} %broadcast_compare_fusion.1), kind=kOutput, calls=%fused_computation.20 | convolution fusion | flops 1612709888 | bytes 6883328 | tf_op jit(solution)/shard_map/cond/branch_1_fun/hmqk,khd->hmqd/dot_general | solution.py:34
  164.1 0.0 copy-start.7
  164.1 0.0 copy-start.6
  164.1 0.0 reduce-scatter.2.cloned.1.call-done
  164.2 1.5 fusion.69
  165.6 1.5 fusion.68
  167.1 1.5 fusion.67
  168.6 1.5 fusion.66
  170.0 1.5 fusion.65
  171.5 1.5 fusion.64
  172.9 1.5 fusion.63
  174.4 1.5 fusion.62
  175.9 3.5 %all-to-all-start.1 = ((bf16[8,1024,32]{1,2,0:T(8,128)(2,1)}), bf16[8,1024,32]{1,2,0:T(8,128)(2,1)S(1)}, u32[]{:S(2)}, u32[]{:S(2)}) async-start(bf16[8,1024,32]{1,2,0:T(8,128)(2,1)} %fusion.62), calls=%async_computation.2 | async-start | bytes 1048576 | tf_op jit(solution)/shard_map/all_to_all | solution.py:144
  179.4 0.3 multiply_reduce_fusion.1
  179.8 0.1 fusion.60
  179.9 0.7 pad_maximum_fusion
  180.7 12.6 %all-to-all-done.1 = bf16[8,1024,32]{1,2,0:T(8,128)(2,1)S(1)} async-done(((bf16[8,1024,32]{1,2,0:T(8,128)(2,1)}), bf16[8,1024,32]{1,2,0:T(8,128)(2,1)S(1)}, u32[]{:S(2)}, u32[]{:S(2)}) %all-to-all-start.1) | async-done | bytes 524320 | tf_op jit(solution)/shard_map/all_to_all | solution.py:144
  193.2 0.2 convolution_multiply_fusion.1
  193.5 0.9 fusion.41
  (33 shorter events, 0.2 us)
Async XLA Ops:
  8.0 6.0 %copy-start.2 = (bf16[64,4096]{1,0:T(8,128)(2,1)S(1)}, bf16[64,4096]{1,0:T(8,128)(2,1)}, u32[]{:S(2)}) copy-start(bf16[64,4096]{1,0:T(8,128)(2,1)} %param.21) | copy-start | bytes 1572868
  8.0 101.8 %all-gather.5.cloned.1.call-start = ((), (), s32[]{:S(2)}) async-start(), calls=%async_computation.4 | async-start | bytes 2359296 | tf_op jit(solution)/shard_map/all_gather | solution.py:77
  18.1 7.5 %copy-start.3 = (bf16[128,1024]{1,0:T(8,128)(2,1)S(1)}, bf16[128,1024]{1,0:T(8,128)(2,1)}, u32[]{:S(2)}) copy-start(bf16[128,1024]{1,0:T(8,128)(2,1)} %param.17) | copy-start | bytes 786436
  18.1 78.2 %all-to-all-start = ((bf16[8,32,4096]{2,1,0:T(8,128)(2,1)}), bf16[8,32,4096]{2,1,0:T(8,128)(2,1)S(1)}, u32[]{:S(2)}, u32[]{:S(2)}) async-start(bf16[8,32,4096]{2,1,0:T(8,128)(2,1)} %bitcast.20), calls=%async_computation | async-start | bytes 4194304 | tf_op jit(solution)/shard_map/all_to_all | solution.py:131
  25.5 121.9 %all-gather.3.cloned.1.call-start = ((), (), s32[]{:S(2)}) async-start(), calls=%async_computation.3 | async-start | bytes 2359296 | tf_op jit(solution)/shard_map/all_gather | solution.py:76
  26.5 137.7 %reduce-scatter.2.cloned.1.call-start = ((), (), s32[]{:S(2)}) async-start(), calls=%async_computation.5 | async-start | bytes 2621440 | tf_op jit(solution)/shard_map/reduce_scatter | solution.py:135
  107.0 2.6 %copy-start.5 = (f32[64,2]{0,1:T(2,128)S(1)}, f32[64,2]{0,1:T(2,128)}, u32[]{:S(2)}) copy-start(f32[64,2]{0,1:T(2,128)} %param.24) | copy-start | bytes 1540
  109.8 37.7 %copy-start.4 = (bf16[128,1024]{1,0:T(8,128)(2,1)S(1)}, bf16[128,1024]{1,0:T(8,128)(2,1)}, u32[]{:S(2)}) copy-start(bf16[128,1024]{1,0:T(8,128)(2,1)} %param.16) | copy-start | bytes 786436
  147.7 3.2 %copy-start = (f32[1024,4,256]{0,2,1:T(8,128)S(1)}, f32[1024,4,256]{0,2,1:T(8,128)}, u32[]{:S(2)}) copy-start(f32[1024,4,256]{0,2,1:T(8,128)} %get-tuple-element.48) | copy-start | bytes 12582916 | tf_op jit(solution)/shard_map/cond
  156.1 3.2 %copy-start.1 = (f32[1024,4,256]{0,2,1:T(8,128)S(1)}, f32[1024,4,256]{0,2,1:T(8,128)}, u32[]{:S(2)}) copy-start(f32[1024,4,256]{0,2,1:T(8,128)} %get-tuple-element.53) | copy-start | bytes 12582916 | tf_op jit(solution)/shard_map/cond
  164.1 15.3 %copy-start.7 = (f32[4]{0:T(128)S(1)}, f32[4]{0:T(128)}, u32[]{:S(2)}) copy-start(f32[4]{0:T(128)} %param.19) | copy-start | bytes 52
  164.1 15.6 %copy-start.6 = (f32[256]{0:T(256)S(1)}, f32[256]{0:T(256)}, u32[]{:S(2)}) copy-start(f32[256]{0:T(256)} %param.20) | copy-start | bytes 3076
  175.9 17.4 %all-to-all-start.1 = ((bf16[8,1024,32]{1,2,0:T(8,128)(2,1)}), bf16[8,1024,32]{1,2,0:T(8,128)(2,1)S(1)}, u32[]{:S(2)}, u32[]{:S(2)}) async-start(bf16[8,1024,32]{1,2,0:T(8,128)(2,1)} %fusion.62), calls=%async_computation.2 | async-start | bytes 1048576 | tf_op jit(solution)/shard_map/all_to_all | solution.py:144
Sparse Core Ops, SparseCore 0:
  10.9 83.9 all-gather.4
  97.4 49.9 all-gather.2
Sparse Core Ops, SparseCore 1:
  107.1 30.1 reduce-scatter.1
